TPU v7x, 32 devices: a whole 2x2x4 slice. The times are simulated.
32 devices in a mesh: grp: 2 (over x), ep: 4 (over y, core), tp: 4 (over z).
Axes of the slice: x: 2, y: 2, z: 4, core: 2. Of those that a mesh axis runs over, the one named last changes fastest.
Arguments:
- tokens: bfloat16 [512, 2048], P(('grp', 'ep')), parts along dimension 0, may hold values from -6 to 6
- routing: int32 [512, 4], P(('grp', 'ep')), parts along dimension 0, may hold values from 0 to 7, all different within a row; in each aligned block of 64 rows (0 to 63, 64 to 127, ...) at most 64 rows name the same one
- route_weight: float32 [512, 4], P(('grp', 'ep')), parts along dimension 0, may hold values from 0.1 to 1
- norm_gain: float32 [2048], replicated, may hold values from 0.1 to 1.9
- gate_weight: bfloat16 [8, 2048, 2048], P('ep', None, 'tp'), may hold values from -2.1213203 to 2.1213203
- up_weight: bfloat16 [8, 2048, 2048], P('ep', None, 'tp'), may hold values from -2.1213203 to 2.1213203
- down_weight: bfloat16 [8, 2048, 2048], P('ep', 'tp'), may hold values from -3.9774756 to 3.9774756
- out_gain: float32 [2048], P('tp'), may hold values from 0.1 to 1.9
Outputs:
- layer_output: bfloat16 [512, 2048], P(('grp', 'ep'), 'tp'), parts along dimension 0
There are 2 independent parts, one for each index of `grp`. A program takes and returns all parts, laid end to end along the dimension named above; an argument that names none is the same for every part. Nothing has to cross between parts.
Inputs may be any that keep to these rules, and one draw needn't show every extreme that they name: `routing`: each row names 4 different experts; among the 64 rows of one index of ep no expert is named more than 64 times, and in some such blocks one expert is named exactly 64 times.
All inputs are finite; a program needn't handle non-finite values.
Results may differ from a plain program's by a relative error of at most 0.017.
Values may be sent and summed in bfloat16 or wider, within the bound.
A program may use at most 64 MiB of HBM per device.

v0:
```python
import functools

import jax
import jax.numpy as jnp
from jax import lax
from jax.experimental import pallas as pl
from jax.experimental.pallas import tpu as pltpu
from jax.sharding import PartitionSpec as P

LIMIT = 7.0
ALPHA = 1.702
EPS = 1e-06
LANES = 128
PIECES = 4
MESH = pl.DeviceIdType.MESH
BF16 = jnp.bfloat16
F32 = jnp.float32


def kernel(
    ep_size,
    tp_size,
    tok_hbm,
    route_hbm,
    weight_hbm,
    gain_hbm,
    out_gain_hbm,
    gate_hbm,
    up_hbm,
    down_hbm,
    out_ref,
    tok_ref,
    route_ref,
    weight_ref,
    gain_ref,
    out_gain_ref,
    rows,
    gate_buf,
    up_buf,
    down_buf,
    hidden,
    core_out,
    core_in,
    core_sum,
    own_sum,
    near_sum,
    late_sum,
    chip_out,
    chip_in,
    early_out,
    early_in,
    late_out,
    late_in,
    back_out,
    back_in,
    feat_out,
    feat_in,
    square_out,
    square_in,
    small_sem,
    load_sem,
    pair_send,
    pair_recv,
    chip_send,
    chip_recv,
    side_send,
    side_recv,
    fwd_send,
    fwd_recv,
    core_send,
    core_recv,
    red_send,
    red_recv,
    early_send,
    early_recv,
    late_send,
    late_recv,
    back_send,
    back_recv,
    feat_send,
    feat_recv,
    sq_send,
    sq_recv,
):
    me, tp = lax.axis_index("ep"), lax.axis_index("tp")
    core = lax.rem(me, 2)
    chip = lax.div(me, 2)
    partner = me + 1 - 2 * core
    chips = ep_size // 2
    toks, width = tok_ref.shape
    code = rows.shape[2] - width
    half = code // 2
    experts, _, ff = gate_buf.shape
    out_width = width // tp_size

    def chip_at(step):
        return lax.rem(chip + step, chips)

    def tp_at(step):
        return lax.rem(tp + step, tp_size)

    def send(src, dst, send_sem, recv_sem, device):
        copy = pltpu.make_async_remote_copy(
            src_ref=src,
            dst_ref=dst,
            send_sem=send_sem,
            recv_sem=recv_sem,
            device_id=device,
            device_id_type=MESH,
        )
        return copy

    sent = []

    def start(*args):
        copy = send(*args)
        copy.start()
        sent.append(copy)

    loads = []
    for e in range(experts):
        for i, (src, dst) in enumerate(((gate_hbm, gate_buf), (up_hbm, up_buf))):
            loads.append((src.at[e], dst.at[e]))
    for e in range(experts):
        loads.append((down_hbm.at[e], down_buf.at[pl.ds(e * ff, ff)]))
    loads = [
        pltpu.make_async_copy(src, dst, load_sem.at[i]) for i, (src, dst) in enumerate(loads)
    ]
    barrier = pltpu.get_barrier_semaphore()
    friends = [{"ep": partner}]
    friends += [{"ep": 2 * chip_at(step) + core} for step in range(1, chips)]
    friends += [{"tp": tp_at(step)} for step in range(1, tp_size)]
    smalls = (
        (tok_hbm, tok_ref),
        (route_hbm, route_ref),
        (weight_hbm, weight_ref),
        (gain_hbm, gain_ref),
        (out_gain_hbm, out_gain_ref),
    )
    smalls = [
        pltpu.make_async_copy(src, dst, small_sem.at[i]) for i, (src, dst) in enumerate(smalls)
    ]
    for load in smalls:
        load.start()
    for friend in friends:
        pl.semaphore_signal(barrier, inc=1, device_id=friend, device_id_type=MESH)
    for load in loads:
        load.start()

    for load in smalls:
        load.wait()
    place = lax.broadcasted_iota(jnp.int32, (code, toks), 0)
    place = jnp.where(place < half, place, place - half)
    placed = jnp.zeros((code, toks), F32)
    for k in range(route_ref.shape[0]):
        placed = placed + jnp.where(place == route_ref[k : k + 1], weight_ref[k : k + 1], 0.0)
    placed = placed.T
    high = placed.astype(BF16).astype(F32)
    first = lax.broadcasted_iota(jnp.int32, (toks, code), 1) < half
    rows[me, :, width:] = jnp.where(first, high, placed - high).astype(BF16)
    scaled = tok_ref[...].astype(F32)
    scale = lax.rsqrt(jnp.mean(scaled * scaled, axis=-1, keepdims=True) + EPS)
    rows[me, :, :width] = (scaled * scale * gain_ref[...]).astype(BF16)

    pl.semaphore_wait(barrier, len(friends))

    odd = lax.rem(tp, 2)
    beside = {"tp": tp + 1 - 2 * odd}
    depth = toks // PIECES
    edge, other_edge = odd * (PIECES - 1), (1 - odd) * (PIECES - 1)

    def piece(slot, p):
        return rows.at[slot, pl.ds(pl.multiple_of(p * depth, depth), depth)]

    direct = [edge] + list(range(1, PIECES - 1))
    for i, p in enumerate(direct):
        for step in range(1, chips):
            block = piece(me, p)
            start(
                block,
                block,
                chip_send.at[step, i],
                chip_recv.at[step, i],
                {"ep": 2 * chip_at(step) + core},
            )
    start(rows.at[me], rows.at[me], pair_send, pair_recv, {"ep": partner})

    def arrived(slot, sem):
        send(slot, slot, pair_send, sem, {"ep": partner}).wait_recv()

    def run_expert(index, e, waits):
        x = rows[pl.ds(2 * index, 2)].reshape(2 * toks, width + code)
        codes = x[:, width:].astype(F32)
        x = x[:, :width]
        lane = lax.broadcasted_iota(jnp.int32, codes.shape, 1)
        lane = jnp.where(lane < half, lane, lane - half)
        mix = jnp.sum(jnp.where(lane == me * experts + e, codes, 0.0), axis=1, keepdims=True)
        if waits:
            loads[2 * e].wait()
        gate = jnp.minimum(jnp.dot(x, gate_buf[e], preferred_element_type=F32), LIMIT)
        if waits:
            loads[2 * e + 1].wait()
        up = jnp.clip(jnp.dot(x, up_buf[e], preferred_element_type=F32), -LIMIT, LIMIT)
        act = (up + 1.0) * gate * jax.nn.sigmoid(ALPHA * gate) * mix
        hidden[pl.ds(2 * index, 2), :, e * ff : (e + 1) * ff] = act.astype(BF16).reshape(
            2, toks, ff
        )

    pieces = direct + [other_edge]

    def forward(i):
        for step in range(1, chips):
            block = piece(2 * chip_at(chips - step) + core, pieces[i])
            if i < len(direct):
                arrived(block, chip_recv.at[step, i])
            else:
                arrived(block, side_recv.at[step])
            if i == 0:
                start(block, block, side_send.at[step], side_recv.at[step], beside)
            start(block, block, fwd_send.at[step, i], fwd_recv.at[step, i], {"ep": partner})

    order = list(range(tp_size // 2, tp_size)) + list(range(1, tp_size // 2))[::-1] + [0]
    cut = out_width // 2

    def project(step, k):
        index = chip_at(step)
        both = jnp.concatenate([hidden[2 * index + 1 - core], hidden[2 * index + core]], axis=0)
        columns = pl.ds(pl.multiple_of(tp_at(k) * out_width, out_width), out_width)
        out = jnp.dot(both, down_buf[:, columns], preferred_element_type=F32)
        core_out[step, k] = out[:toks].astype(BF16)
        core_sum[step, k] = out[toks:]
        start(
            core_out.at[step, k],
            core_in.at[step, k],
            core_send.at[step, k],
            core_recv.at[step, k],
            {"ep": partner},
        )

    def crossed(step, k):
        block = core_in.at[step, k]
        arrived(block, core_recv.at[step, k])
        return core_sum[step, k] + block[...].astype(F32)

    def own_chip(k):
        total = crossed(0, k)
        own_sum[k] = total[:, :cut]
        if k:
            early_out[k - 1] = total[:, cut:].astype(BF16)
            start(
                early_out.at[k - 1],
                early_in.at[k - 1],
                early_send.at[k - 1],
                early_recv.at[k - 1],
                {"tp": tp_at(k)},
            )
        else:
            near_sum[...] = total[:, cut:]

    def other_chip(step, k):
        total = crossed(step, k)
        slot = step - 1
        chip_out[k, slot] = total[:, :cut].astype(BF16)
        start(
            chip_out.at[k, slot],
            chip_in.at[k, slot],
            red_send.at[k, slot],
            red_recv.at[k, slot],
            {"ep": 2 * chip_at(step) + core},
        )
        if k:
            late_out[slot, k - 1] = total[:, cut:].astype(BF16)
            start(
                late_out.at[slot, k - 1],
                late_in.at[slot, k - 1],
                late_send.at[slot, k - 1],
                late_recv.at[slot, k - 1],
                {"tp": tp_at(k)},
            )
        else:
            late_sum[slot] = total[:, cut:]

    arrived(rows.at[partner], pair_recv)
    run_expert(chip, 0, True)
    forward(0)
    for e in range(1, experts):
        run_expert(chip, e, True)
    for i in range(1, len(pieces) - 1):
        forward(i)
        if i == 1:
            for e in range(experts):
                loads[2 * experts + e].wait()
            for k in order:
                project(0, k)
    forward(len(pieces) - 1)
    for k in order:
        own_chip(k)
    for step in range(1, chips):
        index = chip_at(chips - step)
        for i, p in enumerate(pieces):
            arrived(piece(2 * index + 1 - core, p), fwd_recv.at[step, i])
        for e in range(experts):
            run_expert(index, e, False)
        for i, k in enumerate(order):
            project(chips - step, k)
            if i:
                other_chip(chips - step, order[i - 1])
        other_chip(chips - step, order[-1])

    for k in order:
        total = own_sum[k]
        for slot in range(chips - 1):
            block = chip_in.at[k, slot]
            arrived(block, red_recv.at[k, slot])
            total = total + block[...].astype(F32)
        if k:
            feat_out[k - 1] = total.astype(BF16)
            start(
                feat_out.at[k - 1],
                feat_in.at[k - 1],
                feat_send.at[k - 1],
                feat_recv.at[k - 1],
                {"tp": tp_at(k)},
            )
        else:
            left = total
    for slot in range(chips - 1):
        total = late_sum[slot]
        for k in range(1, tp_size):
            block = late_in.at[slot, k - 1]
            arrived(block, late_recv.at[slot, k - 1])
            total = total + block[...].astype(F32)
        back_out[slot] = total.astype(BF16)
        start(
            back_out.at[slot],
            back_in.at[slot],
            back_send.at[slot],
            back_recv.at[slot],
            {"ep": 2 * chip_at(slot + 1) + core},
        )
    right = near_sum[...]
    for k in range(1, tp_size):
        block = early_in.at[k - 1]
        arrived(block, early_recv.at[k - 1])
        right = right + block[...].astype(F32)
    for k in range(1, tp_size):
        block = feat_in.at[k - 1]
        arrived(block, feat_recv.at[k - 1])
        left = left + block[...].astype(F32)
    for slot in range(chips - 1):
        block = back_in.at[slot]
        arrived(block, back_recv.at[slot])
        right = right + block[...].astype(F32)
    mixed = jnp.concatenate([left, right], axis=1)

    squares = mixed * mixed
    folded = jnp.zeros((toks, LANES), F32)
    for j in range(out_width // LANES):
        folded = folded + squares[:, j * LANES : (j + 1) * LANES]
    wide = square_out.shape[1]
    if wide > toks:
        folded = jnp.concatenate([folded, jnp.zeros((wide - toks, LANES), F32)], axis=0)
    line = jnp.sum(folded.T, axis=0, keepdims=True)
    square_out[...] = jnp.broadcast_to(line, square_out.shape)
    for k in range(1, tp_size):
        start(square_out, square_in.at[k - 1], sq_send.at[k - 1], sq_recv.at[k - 1], {"tp": tp_at(k)})
    for k in range(1, tp_size):
        block = square_in.at[k - 1]
        arrived(block, sq_recv.at[k - 1])
        line = line + block[0:1, :]
    total = jnp.broadcast_to(line, (LANES, wide)).T[:toks, :1]
    factor = lax.rsqrt(total / width + EPS)
    out_ref[...] = (mixed * factor * out_gain_ref[...]).astype(BF16)
    for copy in sent:
        copy.wait_send()


def on_device(
    tokens, routing, route_weight, norm_gain, gate_weight, up_weight, down_weight, out_gain
):
    toks, width = tokens.shape
    experts, _, ff = gate_weight.shape
    ep_size, tp_size = lax.axis_size("ep"), lax.axis_size("tp")
    chips = ep_size // 2
    code = 2 * pl.cdiv(experts * ep_size, LANES // 2) * (LANES // 2)
    wide = pl.cdiv(toks, LANES) * LANES
    out_width = width // tp_size
    cut = out_width // 2
    vmem = pl.BlockSpec(memory_space=pltpu.VMEM)
    hbm = pl.BlockSpec(memory_space=pl.ANY)
    dma = pltpu.SemaphoreType.DMA
    return pl.pallas_call(
        functools.partial(kernel, ep_size, tp_size),
        out_shape=pltpu.VMEM((toks, out_width), BF16),
        in_specs=[hbm] * 8,
        out_specs=vmem,
        scratch_shapes=[
            pltpu.VMEM(tokens.shape, tokens.dtype),
            pltpu.VMEM(routing.shape[::-1], routing.dtype),
            pltpu.VMEM(routing.shape[::-1], F32),
            pltpu.VMEM((1, width), F32),
            pltpu.VMEM((1, out_width), F32),
            pltpu.VMEM((ep_size, toks, width + code), BF16),
            pltpu.VMEM((experts, width, ff), BF16),
            pltpu.VMEM((experts, width, ff), BF16),
            pltpu.VMEM((experts * ff, width), BF16),
            pltpu.VMEM((ep_size, toks, experts * ff), BF16),
            pltpu.VMEM((chips, tp_size, toks, out_width), BF16),
            pltpu.VMEM((chips, tp_size, toks, out_width), BF16),
            pltpu.VMEM((chips, tp_size, toks, out_width), F32),
            pltpu.VMEM((tp_size, toks, cut), F32),
            pltpu.VMEM((toks, cut), F32),
            pltpu.VMEM((chips - 1, toks, cut), F32),
            pltpu.VMEM((tp_size, chips - 1, toks, cut), BF16),
            pltpu.VMEM((tp_size, chips - 1, toks, cut), BF16),
            pltpu.VMEM((tp_size - 1, toks, cut), BF16),
            pltpu.VMEM((tp_size - 1, toks, cut), BF16),
            pltpu.VMEM((chips - 1, tp_size - 1, toks, cut), BF16),
            pltpu.VMEM((chips - 1, tp_size - 1, toks, cut), BF16),
            pltpu.VMEM((chips - 1, toks, cut), BF16),
            pltpu.VMEM((chips - 1, toks, cut), BF16),
            pltpu.VMEM((tp_size - 1, toks, cut), BF16),
            pltpu.VMEM((tp_size - 1, toks, cut), BF16),
            pltpu.VMEM((8, wide), F32),
            pltpu.VMEM((tp_size - 1, 8, wide), F32),
            dma((5,)),
            dma((3 * experts,)),
            dma,
            dma,
            dma((chips, PIECES)),
            dma((chips, PIECES)),
            dma((chips,)),
            dma((chips,)),
            dma((chips, PIECES)),
            dma((chips, PIECES)),
            dma((chips, tp_size)),
            dma((chips, tp_size)),
            dma((tp_size, chips - 1)),
            dma((tp_size, chips - 1)),
            dma((tp_size - 1,)),
            dma((tp_size - 1,)),
            dma((chips - 1, tp_size - 1)),
            dma((chips - 1, tp_size - 1)),
            dma((chips - 1,)),
            dma((chips - 1,)),
            dma((tp_size - 1,)),
            dma((tp_size - 1,)),
            dma((tp_size - 1,)),
            dma((tp_size - 1,)),
        ],
        compiler_params=pltpu.CompilerParams(
            collective_id=0, has_side_effects=True, vmem_limit_bytes=60 * 1024 * 1024
        ),
    )(
        tokens,
        routing.T,
        route_weight.T,
        norm_gain.reshape(1, width),
        out_gain.reshape(1, out_width),
        gate_weight,
        up_weight,
        down_weight,
    )


def solution(mesh):
    in_specs = (
        P(("grp", "ep"), None),
        P(("grp", "ep"), None),
        P(("grp", "ep"), None),
        P(),
        P("ep", None, "tp"),
        P("ep", None, "tp"),
        P("ep", "tp", None),
        P("tp"),
    )
    out_specs = P(("grp", "ep"), "tp")
    return jax.shard_map(
        on_device, mesh=mesh, in_specs=in_specs, out_specs=out_specs, check_vma=False
    )
```

profile of v0, /device:TPU:0, one launch (start us, length us, event | category | flops | bytes accessed | tf_op | source)
XLA Modules:
  0.0 28.9 jit_solution(8699782114069585410)
XLA Ops:
  0.0 28.3 %shard_map.82 = bf16[64,512]{1,0:T(8,128)(2,1)S(1)} custom-call(bf16[64,2048]{1,0:T(8,128)(2,1)} %tok_hbm.1, s32[4,64]{1,0:T(4,128)} %bitcast.5, f32[4,64]{1,0:T(4,128)} %bitcast.6, f32[1,2048]{1,0:T(1,128)} %bitcast.4, f32[1,512]{1,0:T(1,128)} %bitcast.7, bf16[2,2048,512]{2,1,0:T(8,128)(2,1)} %gate_hbm.1, bf16[2,2048,512]{2,1,0:T(8,128)(2,1)} %up_hbm.1, ...), custom_call_target="tpu_custom_call" | custom-call | tf_op jit(solution)/shard_map/pallas_call | solution.py:392
  28.3 0.6 %copy.10 = bf16[64,512]{1,0:T(8,128)(2,1)} copy(bf16[64,512]{1,0:T(8,128)(2,1)S(1)} %shard_map.82) | data formatting | bytes 131072
where the time goes:
time: 29.1 us; the launch traced here: 28.9 us
  Pallas kernels  28.3 us (97%)
  local copies, waits for them, and re-layouts  0.63 us (2%)
    pallas_call x1, Pallas kernels, on_device(): pl.pallas_call(functools.partial(kernel, ep_size, tp_size), out_shape=plt...  28.3 us
    unnamed x1, local copies, waits for them, and re-layouts  0.63 us

commit v1 on v0

v1 whole, which is shorter than its diff:
```python
import functools

import jax
import jax.numpy as jnp
from jax import lax
from jax.experimental import pallas as pl
from jax.experimental.pallas import tpu as pltpu
from jax.sharding import PartitionSpec as P

LIMIT = 7.0
ALPHA = 1.702
EPS = 1e-06
LANES = 128
PIECES = 8
SIDE = 2
CHUNKS = ((0, 4), (4, 8))
MESH = pl.DeviceIdType.MESH
BF16 = jnp.bfloat16
F32 = jnp.float32


def kernel(
    ep_size,
    tp_size,
    tok_hbm,
    route_hbm,
    weight_hbm,
    gain_hbm,
    out_gain_hbm,
    gate_hbm,
    up_hbm,
    down_hbm,
    out_ref,
    tok_ref,
    route_ref,
    weight_ref,
    gain_ref,
    out_gain_ref,
    rows,
    codes,
    gu_buf,
    down_buf,
    acc,
    hidden,
    core_out,
    core_in,
    core_sum,
    own_sum,
    near_sum,
    late_sum,
    chip_out,
    chip_in,
    early_out,
    early_in,
    late_out,
    late_in,
    back_out,
    back_in,
    feat_out,
    feat_in,
    square_out,
    square_in,
    small_sem,
    load_sem,
    ready,
    sent_sem,
    pair_recv,
    code_recv,
    chip_recv,
    side_recv,
    fwd_recv,
    core_recv,
    red_recv,
    early_recv,
    late_recv,
    back_recv,
    feat_recv,
    sq_recv,
):
    me, tp = lax.axis_index("ep"), lax.axis_index("tp")
    core = lax.rem(me, 2)
    chip = lax.div(me, 2)
    odd = lax.rem(tp, 2)
    partner = me + 1 - 2 * core
    beside = {"tp": tp + 1 - 2 * odd}
    chips = ep_size // 2
    toks, width = tok_ref.shape
    experts, _, _, ff = gu_buf.shape
    out_width = width // tp_size
    cut = out_width // 2
    depth = width // PIECES
    direct = PIECES - SIDE

    def chip_at(step):
        return lax.rem(chip + step, chips)

    def tp_at(step):
        return lax.rem(tp + step, tp_size)

    def send(src, dst, send_sem, recv_sem, device):
        return pltpu.make_async_remote_copy(
            src_ref=src,
            dst_ref=dst,
            send_sem=send_sem,
            recv_sem=recv_sem,
            device_id=device,
            device_id_type=MESH,
        )

    sent = []

    def start(src, dst, recv_sem, device):
        copy = send(src, dst, sent_sem, recv_sem, device)
        copy.start()
        sent.append(copy)

    def arrived(slot, sem):
        send(slot, slot, sent_sem, sem, {"ep": partner}).wait_recv()

    def tell(sem):
        @pl.when(tp > 0)
        def _():
            pl.semaphore_signal(sem, inc=1, device_id={"tp": tp - 1}, device_id_type=MESH)

        @pl.when(tp < tp_size - 1)
        def _():
            pl.semaphore_signal(sem, inc=1, device_id={"tp": tp + 1}, device_id_type=MESH)

    beside_count = lax.div(tp + tp_size - 1, tp_size) + lax.div(2 * tp_size - 2 - tp, tp_size)

    loads = []
    for e in range(experts):
        loads.append((gate_hbm.at[e], gu_buf.at[e, 0], e))
        loads.append((up_hbm.at[e], gu_buf.at[e, 1], e))
    for e in range(experts):
        loads.append((down_hbm.at[e], down_buf.at[pl.ds(e * ff, ff)], experts))
    loads = [pltpu.make_async_copy(src, dst, load_sem.at[i]) for src, dst, i in loads]

    def loaded(slot, i):
        pltpu.make_async_copy(slot, slot, load_sem.at[i]).wait()

    smalls = (
        (tok_hbm, tok_ref),
        (gain_hbm, gain_ref),
        (route_hbm, route_ref),
        (weight_hbm, weight_ref),
        (out_gain_hbm, out_gain_ref),
    )
    smalls = [
        pltpu.make_async_copy(src, dst, small_sem.at[i]) for i, (src, dst) in enumerate(smalls)
    ]
    barrier = pltpu.get_barrier_semaphore()
    for load in smalls:
        load.start()
    for step in range(1, ep_size):
        pl.semaphore_signal(
            barrier, inc=1, device_id={"ep": lax.rem(me + step, ep_size)}, device_id_type=MESH
        )
    tell(barrier)
    for load in loads:
        load.start()

    for load in smalls[:2]:
        load.wait()
    scaled = tok_ref[...].astype(F32)
    scale = lax.rsqrt(jnp.mean(scaled * scaled, axis=-1, keepdims=True) + EPS)
    scaled = (scaled * scale * gain_ref[...]).astype(BF16)
    for p in range(PIECES):
        rows[me, p] = scaled[:, p * depth : (p + 1) * depth]

    pl.semaphore_wait(barrier, ep_size - 1 + beside_count)

    def piece(slot, j):
        return rows.at[slot, j + odd * (PIECES - 1 - 2 * j)]

    for j in range(direct):
        for step in range(1, chips):
            block = piece(me, j)
            start(block, block, chip_recv.at[step - 1, j], {"ep": 2 * chip_at(step) + core})
        if j == 0:
            start(rows.at[me], rows.at[me], pair_recv, {"ep": partner})
    if tp_size > 2:
        tell(ready.at[0])

    for load in smalls[2:4]:
        load.wait()
    place = lax.broadcasted_iota(jnp.int32, (codes.shape[1], toks), 0)
    placed = jnp.zeros(place.shape, F32)
    for k in range(route_ref.shape[0]):
        placed = placed + jnp.where(place == route_ref[k : k + 1], weight_ref[k : k + 1], 0.0)
    codes[me] = jnp.zeros(codes.shape[1:], F32)
    codes[me, :, :toks] = placed
    start(codes.at[me], codes.at[me], code_recv.at[0], {"ep": partner})
    for step in range(1, chips):
        for other in range(2):
            start(
                codes.at[me],
                codes.at[me],
                code_recv.at[1],
                {"ep": 2 * chip_at(step) + other},
            )

    def mixes(index):
        columns = jnp.concatenate([codes[2 * index + c].T[:toks] for c in range(2)], axis=0)
        lane = lax.broadcasted_iota(jnp.int32, columns.shape, 1)
        return [
            jnp.sum(jnp.where(lane == me * experts + e, columns, 0.0), axis=1, keepdims=True)
            for e in range(experts)
        ]

    def features(index, first, count):
        both = pl.ds(2 * index, 2)
        parts = [rows[both, first + t].reshape(2 * toks, depth) for t in range(count)]
        return jnp.concatenate(parts, axis=1)

    def activate(index, e, gate, up, mix):
        gate = jnp.minimum(gate, LIMIT)
        up = jnp.clip(up, -LIMIT, LIMIT)
        act = (up + 1.0) * gate * jax.nn.sigmoid(ALPHA * gate) * mix
        act = act.astype(BF16).reshape(2, toks, ff)
        hidden[pl.ds(2 * index, 2), :, e * ff : (e + 1) * ff] = act

    def own_expert(e, mix):
        x = features(chip, 0, PIECES)
        loaded(gu_buf.at[e], e)
        gate = jnp.dot(x, gu_buf[e, 0], preferred_element_type=F32)
        up = jnp.dot(x, gu_buf[e, 1], preferred_element_type=F32)
        activate(chip, e, gate, up, mix)

    def other_experts(index, number, mix):
        a, b = CHUNKS[number]
        first = a + odd * (PIECES - a - b)
        x = features(index, first, b - a)
        part = pl.ds(pl.multiple_of(first * depth, depth), (b - a) * depth)
        for e in range(experts):
            sums = []
            for i in range(2):
                total = jnp.dot(x, gu_buf[e, i, part, :], preferred_element_type=F32)
                if number:
                    total = total + acc[e, i]
                sums.append(total)
            if number == len(CHUNKS) - 1:
                activate(index, e, sums[0], sums[1], mix[e])
            else:
                for i in range(2):
                    acc[e, i] = sums[i]

    def forward(j):
        number = [a <= j < b for a, b in CHUNKS].index(True)
        for step in range(1, chips):
            block = piece(2 * chip_at(chips - step) + core, j)
            if j < direct:
                arrived(block, chip_recv.at[step - 1, j])
            else:
                arrived(block, side_recv.at[step - 1, j - direct])
            if j < SIDE:
                start(block, block, side_recv.at[step - 1, SIDE - 1 - j], beside)
            start(block, block, fwd_recv.at[step - 1, number], {"ep": partner})

    order = list(range(tp_size // 2, tp_size)) + list(range(1, tp_size // 2))[::-1] + [0]

    def project(step, k):
        index = chip_at(step)
        both = jnp.concatenate([hidden[2 * index + 1 - core], hidden[2 * index + core]], axis=0)
        columns = pl.ds(pl.multiple_of(tp_at(k) * out_width, out_width), out_width)
        out = jnp.dot(both, down_buf[:, columns], preferred_element_type=F32)
        core_out[step, k] = out[:toks].astype(BF16)
        core_sum[step, k] = out[toks:]
        start(
            core_out.at[step, k], core_in.at[step, k], core_recv.at[step, k], {"ep": partner}
        )

    def crossed(step, k):
        block = core_in.at[step, k]
        arrived(block, core_recv.at[step, k])
        return core_sum[step, k] + block[...].astype(F32)

    def own_chip(k):
        total = crossed(0, k)
        own_sum[k] = total[:, :cut]
        if k:
            early_out[k - 1] = total[:, cut:].astype(BF16)
            start(early_out.at[k - 1], early_in.at[k - 1], early_recv, {"tp": tp_at(k)})
        else:
            near_sum[...] = total[:, cut:]

    def other_chip(step, k):
        total = crossed(step, k)
        slot = step - 1
        chip_out[k, slot] = total[:, :cut].astype(BF16)
        start(
            chip_out.at[k, slot],
            chip_in.at[k, slot],
            red_recv.at[k, slot],
            {"ep": 2 * chip_at(step) + core},
        )
        if k:
            late_out[slot, k - 1] = total[:, cut:].astype(BF16)
            start(
                late_out.at[slot, k - 1],
                late_in.at[slot, k - 1],
                late_recv.at[slot],
                {"tp": tp_at(k)},
            )
        else:
            late_sum[slot] = total[:, cut:]

    arrived(rows.at[partner], pair_recv)
    arrived(codes.at[partner], code_recv.at[0])
    mix = mixes(chip)
    for e in range(experts):
        own_expert(e, mix[e])
    for r in range(tp_size - 2):
        pl.semaphore_wait(ready.at[r], beside_count)
        if r + 1 < tp_size - 2:
            tell(ready.at[r + 1])
    forward(0)
    loaded(down_buf, experts)
    for i, k in enumerate(order):
        project(0, k)
        if i == len(order) // 2 - 1:
            forward(1)
    forward(2)
    for k in order:
        own_chip(k)
    for j in list(range(3, direct)) + list(range(direct, PIECES))[::-1]:
        forward(j)
    if chips > 1:
        arrived(codes.at[pl.ds(0, ep_size - 2)], code_recv.at[1])
    for step in range(1, chips):
        index = chip_at(chips - step)
        mix = mixes(index)
        for number, (a, b) in enumerate(CHUNKS):
            first = a + odd * (PIECES - a - b)
            block = rows.at[2 * index + 1 - core, pl.ds(first, b - a)]
            arrived(block, fwd_recv.at[step - 1, number])
            other_experts(index, number, mix)
        for k in order:
            project(chips - step, k)
        for k in order:
            other_chip(chips - step, k)

    for k in order:
        total = own_sum[k]
        for slot in range(chips - 1):
            block = chip_in.at[k, slot]
            arrived(block, red_recv.at[k, slot])
            total = total + block[...].astype(F32)
        if k:
            feat_out[k - 1] = total.astype(BF16)
            start(feat_out.at[k - 1], feat_in.at[k - 1], feat_recv, {"tp": tp_at(k)})
        else:
            left = total
    for slot in range(chips - 1):
        total = late_sum[slot]
        arrived(late_in.at[slot], late_recv.at[slot])
        for k in range(1, tp_size):
            total = total + late_in[slot, k - 1].astype(F32)
        back_out[slot] = total.astype(BF16)
        start(
            back_out.at[slot],
            back_in.at[slot],
            back_recv,
            {"ep": 2 * chip_at(slot + 1) + core},
        )
    right = near_sum[...]
    arrived(early_in, early_recv)
    for k in range(1, tp_size):
        right = right + early_in[k - 1].astype(F32)
    arrived(feat_in, feat_recv)
    for k in range(1, tp_size):
        left = left + feat_in[k - 1].astype(F32)
    if chips > 1:
        arrived(back_in, back_recv)
    for slot in range(chips - 1):
        right = right + back_in[slot].astype(F32)
    mixed = jnp.concatenate([left, right], axis=1)

    squares = mixed * mixed
    folded = jnp.zeros((toks, LANES), F32)
    for j in range(out_width // LANES):
        folded = folded + squares[:, j * LANES : (j + 1) * LANES]
    wide = square_out.shape[1]
    if wide > toks:
        folded = jnp.concatenate([folded, jnp.zeros((wide - toks, LANES), F32)], axis=0)
    line = jnp.sum(folded.T, axis=0, keepdims=True)
    square_out[...] = jnp.broadcast_to(line, square_out.shape)
    for k in range(1, tp_size):
        start(square_out, square_in.at[k - 1], sq_recv, {"tp": tp_at(k)})
    arrived(square_in, sq_recv)
    for k in range(1, tp_size):
        line = line + square_in[k - 1, 0:1, :]
    total = jnp.broadcast_to(line, (LANES, wide)).T[:toks, :1]
    factor = lax.rsqrt(total / width + EPS)
    smalls[4].wait()
    out_ref[...] = (mixed * factor * out_gain_ref[...]).astype(BF16)
    for copy in sent:
        copy.wait_send()


def on_device(
    tokens, routing, route_weight, norm_gain, gate_weight, up_weight, down_weight, out_gain
):
    toks, width = tokens.shape
    experts, _, ff = gate_weight.shape
    ep_size, tp_size = lax.axis_size("ep"), lax.axis_size("tp")
    chips = ep_size // 2
    wide = pl.cdiv(toks, LANES) * LANES
    out_width = width // tp_size
    cut = out_width // 2
    vmem = pl.BlockSpec(memory_space=pltpu.VMEM)
    hbm = pl.BlockSpec(memory_space=pl.ANY)
    dma = pltpu.SemaphoreType.DMA
    return pl.pallas_call(
        functools.partial(kernel, ep_size, tp_size),
        out_shape=pltpu.VMEM((toks, out_width), BF16),
        in_specs=[hbm] * 8,
        out_specs=vmem,
        scratch_shapes=[
            pltpu.VMEM(tokens.shape, tokens.dtype),
            pltpu.VMEM(routing.shape[::-1], routing.dtype),
            pltpu.VMEM(routing.shape[::-1], F32),
            pltpu.VMEM((1, width), F32),
            pltpu.VMEM((1, out_width), F32),
            pltpu.VMEM((ep_size, PIECES, toks, width // PIECES), BF16),
            pltpu.VMEM((ep_size, pl.cdiv(experts * ep_size, 8) * 8, wide), F32),
            pltpu.VMEM((experts, 2, width, ff), BF16),
            pltpu.VMEM((experts * ff, width), BF16),
            pltpu.VMEM((experts, 2, 2 * toks, ff), F32),
            pltpu.VMEM((ep_size, toks, experts * ff), BF16),
            pltpu.VMEM((chips, tp_size, toks, out_width), BF16),
            pltpu.VMEM((chips, tp_size, toks, out_width), BF16),
            pltpu.VMEM((chips, tp_size, toks, out_width), F32),
            pltpu.VMEM((tp_size, toks, cut), F32),
            pltpu.VMEM((toks, cut), F32),
            pltpu.VMEM((chips - 1, toks, cut), F32),
            pltpu.VMEM((tp_size, chips - 1, toks, cut), BF16),
            pltpu.VMEM((tp_size, chips - 1, toks, cut), BF16),
            pltpu.VMEM((tp_size - 1, toks, cut), BF16),
            pltpu.VMEM((tp_size - 1, toks, cut), BF16),
            pltpu.VMEM((chips - 1, tp_size - 1, toks, cut), BF16),
            pltpu.VMEM((chips - 1, tp_size - 1, toks, cut), BF16),
            pltpu.VMEM((chips - 1, toks, cut), BF16),
            pltpu.VMEM((chips - 1, toks, cut), BF16),
            pltpu.VMEM((tp_size - 1, toks, cut), BF16),
            pltpu.VMEM((tp_size - 1, toks, cut), BF16),
            pltpu.VMEM((8, wide), F32),
            pltpu.VMEM((tp_size - 1, 8, wide), F32),
            dma((5,)),
            dma((experts + 1,)),
            pltpu.SemaphoreType.REGULAR((tp_size - 2,)),
            dma,
            dma,
            dma((2,)),
            dma((chips - 1, PIECES - SIDE)),
            dma((chips - 1, SIDE)),
            dma((chips - 1, len(CHUNKS))),
            dma((chips, tp_size)),
            dma((tp_size, chips - 1)),
            dma,
            dma((chips - 1,)),
            dma,
            dma,
            dma,
        ],
        compiler_params=pltpu.CompilerParams(
            collective_id=0, has_side_effects=True, vmem_limit_bytes=60 * 1024 * 1024
        ),
    )(
        tokens,
        routing.T,
        route_weight.T,
        norm_gain.reshape(1, width),
        out_gain.reshape(1, out_width),
        gate_weight,
        up_weight,
        down_weight,
    )


def solution(mesh):
    in_specs = (
        P(("grp", "ep"), None),
        P(("grp", "ep"), None),
        P(("grp", "ep"), None),
        P(),
        P("ep", None, "tp"),
        P("ep", None, "tp"),
        P("ep", "tp", None),
        P("tp"),
    )
    out_specs = P(("grp", "ep"), "tp")
    return jax.shard_map(
        on_device, mesh=mesh, in_specs=in_specs, out_specs=out_specs, check_vma=False
    )
```

time: 29.1 us -> 28.2 us (0.969)
  Pallas kernels: 28.3 us -> 27.4 us
    pallas_call x1, Pallas kernels: 28.3 us -> 27.4 us  [on_device(): pl.pallas_call(functools.partial(kernel, ep_size, tp_size), out_shape=plt...]
where the time goes in v1:
time: 28.2 us; the launch traced here: 28 us
  Pallas kernels  27.4 us (97%)
  local copies, waits for them, and re-layouts  0.63 us (2%)
    pallas_call x1, Pallas kernels, on_device(): pl.pallas_call(functools.partial(kernel, ep_size, tp_size), out_shape=plt...  27.4 us
    unnamed x1, local copies, waits for them, and re-layouts  0.63 us

profile of v1, /device:TPU:0, one launch (start us, length us, event | category | flops | bytes accessed | tf_op | source)
XLA Modules:
  0.0 28.0 jit_solution(6539750832849440805)
XLA Ops:
  0.0 27.4 %shard_map.82 = bf16[64,512]{1,0:T(8,128)(2,1)S(1)} custom-call(bf16[64,2048]{1,0:T(8,128)(2,1)} %tok_hbm.1, s32[4,64]{1,0:T(4,128)} %bitcast.5, f32[4,64]{1,0:T(4,128)} %bitcast.6, f32[1,2048]{1,0:T(1,128)} %bitcast.4, f32[1,512]{1,0:T(1,128)} %bitcast.7, bf16[2,2048,512]{2,1,0:T(8,128)(2,1)} %gate_hbm.1, bf16[2,2048,512]{2,1,0:T(8,128)(2,1)} %up_hbm.1, ...), custom_call_target="tpu_custom_call" | custom-call | tf_op jit(solution)/shard_map/pallas_call | solution.py:414
  27.4 0.6 %copy.10 = bf16[64,512]{1,0:T(8,128)(2,1)} copy(bf16[64,512]{1,0:T(8,128)(2,1)S(1)} %shard_map.82) | data formatting | bytes 131072

commit v2 on v1

--- a/solution.py
+++ b/solution.py
@@ -13,7 +13,7 @@
 LANES = 128
 PIECES = 8
 SIDE = 2
-CHUNKS = ((0, 4), (4, 8))
+CHUNKS = ((0, 4), (4, 6), (6, 8))
 MESH = pl.DeviceIdType.MESH
 BF16 = jnp.bfloat16
 F32 = jnp.float32
@@ -126,6 +126,11 @@
         def _():
             pl.semaphore_signal(sem, inc=1, device_id={"tp": tp + 1}, device_id_type=MESH)
 
+    def learn(r):
+        pl.semaphore_wait(ready.at[r], beside_count)
+        if r + 1 < tp_size - 2:
+            tell(ready.at[r + 1])
+
     beside_count = lax.div(tp + tp_size - 1, tp_size) + lax.div(2 * tp_size - 2 - tp, tp_size)
 
     loads = []
@@ -257,7 +262,15 @@
                 start(block, block, side_recv.at[step - 1, SIDE - 1 - j], beside)
             start(block, block, fwd_recv.at[step - 1, number], {"ep": partner})
 
-    order = list(range(tp_size // 2, tp_size)) + list(range(1, tp_size // 2))[::-1] + [0]
+    order = [0] * (tp_size - 1)
+    for t in range(tp_size):
+        here = 1 - lax.div((tp - t) * (tp - t) + tp_size * tp_size - 1, tp_size * tp_size)
+        far = sorted((o for o in range(tp_size) if o != t), key=lambda o: -abs(o - t))
+        order = [k + here * ((o - t) % tp_size) for k, o in zip(order, far)]
+    order.append(0)
+
+    def own(k):
+        return isinstance(k, int)
 
     def project(step, k):
         index = chip_at(step)
@@ -278,7 +291,7 @@
     def own_chip(k):
         total = crossed(0, k)
         own_sum[k] = total[:, :cut]
-        if k:
+        if not own(k):
             early_out[k - 1] = total[:, cut:].astype(BF16)
             start(early_out.at[k - 1], early_in.at[k - 1], early_recv, {"tp": tp_at(k)})
         else:
@@ -294,7 +307,7 @@
             red_recv.at[k, slot],
             {"ep": 2 * chip_at(step) + core},
         )
-        if k:
+        if not own(k):
             late_out[slot, k - 1] = total[:, cut:].astype(BF16)
             start(
                 late_out.at[slot, k - 1],
@@ -310,10 +323,8 @@
     mix = mixes(chip)
     for e in range(experts):
         own_expert(e, mix[e])
-    for r in range(tp_size - 2):
-        pl.semaphore_wait(ready.at[r], beside_count)
-        if r + 1 < tp_size - 2:
-            tell(ready.at[r + 1])
+    if tp_size > 2:
+        learn(0)
     forward(0)
     loaded(down_buf, experts)
     for i, k in enumerate(order):
@@ -321,20 +332,36 @@
         if i == len(order) // 2 - 1:
             forward(1)
     forward(2)
+    forward(3)
+    for r in range(1, tp_size - 2):
+        learn(r)
     for k in order:
         own_chip(k)
-    for j in list(range(3, direct)) + list(range(direct, PIECES))[::-1]:
+    for j in range(4, direct):
         forward(j)
     if chips > 1:
         arrived(codes.at[pl.ds(0, ep_size - 2)], code_recv.at[1])
+
+    def sides():
+        for j in range(PIECES - 1, direct - 1, -1):
+            forward(j)
+
+    sides()
+
+    marked = len(sent)
     for step in range(1, chips):
         index = chip_at(chips - step)
-        mix = mixes(index)
         for number, (a, b) in enumerate(CHUNKS):
             first = a + odd * (PIECES - a - b)
             block = rows.at[2 * index + 1 - core, pl.ds(first, b - a)]
             arrived(block, fwd_recv.at[step - 1, number])
+            if number == 0:
+                mix = mixes(index)
             other_experts(index, number, mix)
+            if number == 0 and step == 1:
+
+                del sent[marked:]
+
         for k in order:
             project(chips - step, k)
         for k in order:
@@ -346,7 +373,7 @@
             block = chip_in.at[k, slot]
             arrived(block, red_recv.at[k, slot])
             total = total + block[...].astype(F32)
-        if k:
+        if not own(k):
             feat_out[k - 1] = total.astype(BF16)
             start(feat_out.at[k - 1], feat_in.at[k - 1], feat_recv, {"tp": tp_at(k)})
         else:

time: 28.2 us -> 27.7 us (0.982)
  Pallas kernels: 27.4 us -> 26.9 us
    pallas_call x1, Pallas kernels: 27.4 us -> 26.9 us  [on_device(): pl.pallas_call(functools.partial(kernel, ep_size, tp_size), out_shape=plt...]
where the time goes in v2:
time: 27.7 us; the launch traced here: 27.6 us
  Pallas kernels  26.9 us (97%)
  local copies, waits for them, and re-layouts  0.63 us (2%)
    pallas_call x1, Pallas kernels, on_device(): pl.pallas_call(functools.partial(kernel, ep_size, tp_size), out_shape=plt...  26.9 us
    unnamed x1, local copies, waits for them, and re-layouts  0.63 us

profile of v2, /device:TPU:0, one launch (start us, length us, event | category | flops | bytes accessed | tf_op | source)
XLA Modules:
  0.0 27.6 jit_solution(3215292506220294026)
XLA Ops:
  0.0 26.9 %shard_map.82 = bf16[64,512]{1,0:T(8,128)(2,1)S(1)} custom-call(bf16[64,2048]{1,0:T(8,128)(2,1)} %tok_hbm.1, s32[4,64]{1,0:T(4,128)} %bitcast.5, f32[4,64]{1,0:T(4,128)} %bitcast.6, f32[1,2048]{1,0:T(1,128)} %bitcast.4, f32[1,512]{1,0:T(1,128)} %bitcast.7, bf16[2,2048,512]{2,1,0:T(8,128)(2,1)} %gate_hbm.1, bf16[2,2048,512]{2,1,0:T(8,128)(2,1)} %up_hbm.1, ...), custom_call_target="tpu_custom_call" | custom-call | tf_op jit(solution)/shard_map/pallas_call | solution.py:441
  27.0 0.6 %copy.10 = bf16[64,512]{1,0:T(8,128)(2,1)} copy(bf16[64,512]{1,0:T(8,128)(2,1)S(1)} %shard_map.82) | data formatting | bytes 131072

commit v3 on v2

--- a/solution.py
+++ b/solution.py
@@ -11,9 +11,9 @@
 ALPHA = 1.702
 EPS = 1e-06
 LANES = 128
-PIECES = 8
-SIDE = 2
-CHUNKS = ((0, 4), (4, 6), (6, 8))
+PIECES = 16
+SIDE = 4
+CHUNKS = ((0, 8), (8, 12), (12, 16))
 MESH = pl.DeviceIdType.MESH
 BF16 = jnp.bfloat16
 F32 = jnp.float32
@@ -63,6 +63,7 @@
     small_sem,
     load_sem,
     ready,
+    turn,
     sent_sem,
     pair_recv,
     code_recv,
@@ -91,8 +92,10 @@
     depth = width // PIECES
     direct = PIECES - SIDE
 
+    chip_table = [lax.rem(chip + step, chips) for step in range(chips)]
+
     def chip_at(step):
-        return lax.rem(chip + step, chips)
+        return chip_table[step]
 
     def tp_at(step):
         return lax.rem(tp + step, tp_size)
@@ -112,7 +115,7 @@
     def start(src, dst, recv_sem, device):
         copy = send(src, dst, sent_sem, recv_sem, device)
         copy.start()
-        sent.append(copy)
+        sent.append(src)
 
     def arrived(slot, sem):
         send(slot, slot, sent_sem, sem, {"ep": partner}).wait_recv()
@@ -178,12 +181,16 @@
     def piece(slot, j):
         return rows.at[slot, j + odd * (PIECES - 1 - 2 * j)]
 
-    for j in range(direct):
-        for step in range(1, chips):
-            block = piece(me, j)
-            start(block, block, chip_recv.at[step - 1, j], {"ep": 2 * chip_at(step) + core})
-        if j == 0:
-            start(rows.at[me], rows.at[me], pair_recv, {"ep": partner})
+    def send_pieces():
+        for j in range(direct):
+            for step in range(1, chips):
+                block = piece(me, j)
+                slot = chip_recv.at[step - 1, j]
+                start(block, block, slot, {"ep": 2 * chip_at(step) + core})
+
+    start(rows.at[me], rows.at[me], pair_recv, {"ep": partner})
+
+    send_pieces()
     if tp_size > 2:
         tell(ready.at[0])
 
@@ -323,21 +330,26 @@
     mix = mixes(chip)
     for e in range(experts):
         own_expert(e, mix[e])
+    forward(0)
+    forward(1)
     if tp_size > 2:
         learn(0)
-    forward(0)
     loaded(down_buf, experts)
     for i, k in enumerate(order):
         project(0, k)
-        if i == len(order) // 2 - 1:
-            forward(1)
-    forward(2)
-    forward(3)
+        if i == len(order) // 4 - 1:
+            forward(2)
+            forward(3)
+        if i == 3 * len(order) // 4 - 1:
+            forward(4)
+            forward(5)
+    forward(6)
+    forward(7)
     for r in range(1, tp_size - 2):
         learn(r)
     for k in order:
         own_chip(k)
-    for j in range(4, direct):
+    for j in range(8, direct):
         forward(j)
     if chips > 1:
         arrived(codes.at[pl.ds(0, ep_size - 2)], code_recv.at[1])
@@ -346,9 +358,12 @@
         for j in range(PIECES - 1, direct - 1, -1):
             forward(j)
 
-    sides()
-
     marked = len(sent)
+
+    @pl.when(core == 1)
+    def _():
+        sides()
+
     for step in range(1, chips):
         index = chip_at(chips - step)
         for number, (a, b) in enumerate(CHUNKS):
@@ -360,24 +375,41 @@
             other_experts(index, number, mix)
             if number == 0 and step == 1:
 
+                @pl.when(core == 0)
+                def _():
+                    sides()
+
                 del sent[marked:]
+                sent.extend([rows.at[me, 0]] * (SIDE * (chips - 1)))
 
         for k in order:
             project(chips - step, k)
+
+        @pl.when(core == 1)
+        def _():
+            pl.semaphore_wait(turn, 1)
+
         for k in order:
             other_chip(chips - step, k)
 
-    for k in order:
+        @pl.when(core == 0)
+        def _():
+            pl.semaphore_signal(turn, inc=1, device_id={"ep": partner}, device_id_type=MESH)
+
+    def reduced(k):
         total = own_sum[k]
         for slot in range(chips - 1):
             block = chip_in.at[k, slot]
             arrived(block, red_recv.at[k, slot])
             total = total + block[...].astype(F32)
-        if not own(k):
-            feat_out[k - 1] = total.astype(BF16)
-            start(feat_out.at[k - 1], feat_in.at[k - 1], feat_recv, {"tp": tp_at(k)})
-        else:
-            left = total
+        return total
+
+    def own_features(k):
+        feat_out[k - 1] = reduced(k).astype(BF16)
+        start(feat_out.at[k - 1], feat_in.at[k - 1], feat_recv, {"tp": tp_at(k)})
+
+    for k in order[:-2]:
+        own_features(k)
     for slot in range(chips - 1):
         total = late_sum[slot]
         arrived(late_in.at[slot], late_recv.at[slot])
@@ -390,6 +422,8 @@
             back_recv,
             {"ep": 2 * chip_at(slot + 1) + core},
         )
+    own_features(order[-2])
+    left = reduced(0)
     right = near_sum[...]
     arrived(early_in, early_recv)
     for k in range(1, tp_size):
@@ -421,8 +455,8 @@
     factor = lax.rsqrt(total / width + EPS)
     smalls[4].wait()
     out_ref[...] = (mixed * factor * out_gain_ref[...]).astype(BF16)
-    for copy in sent:
-        copy.wait_send()
+    for src in sent:
+        send(src, src, sent_sem, sent_sem, {"ep": partner}).wait_send()
 
 
 def on_device(
@@ -476,6 +510,7 @@
             dma((5,)),
             dma((experts + 1,)),
             pltpu.SemaphoreType.REGULAR((tp_size - 2,)),
+            pltpu.SemaphoreType.REGULAR,
             dma,
             dma,
             dma((2,)),

time: 27.7 us -> 26.9 us (0.971)
  Pallas kernels: 26.9 us -> 26.2 us
    pallas_call x1, Pallas kernels: 26.9 us -> 26.2 us  [on_device(): pl.pallas_call(functools.partial(kernel, ep_size, tp_size), out_shape=plt...]
where the time goes in v3:
time: 26.9 us; the launch traced here: 26.8 us
  Pallas kernels  26.2 us (97%)
  local copies, waits for them, and re-layouts  0.63 us (2%)
    pallas_call x1, Pallas kernels, on_device(): pl.pallas_call(functools.partial(kernel, ep_size, tp_size), out_shape=plt...  26.2 us
    unnamed x1, local copies, waits for them, and re-layouts  0.63 us

profile of v3, /device:TPU:0, one launch (start us, length us, event | category | flops | bytes accessed | tf_op | source)
XLA Modules:
  0.0 26.8 jit_solution(2024497933287346953)
XLA Ops:
  0.0 26.2 %shard_map.82 = bf16[64,512]{1,0:T(8,128)(2,1)S(1)} custom-call(bf16[64,2048]{1,0:T(8,128)(2,1)} %tok_hbm.1, s32[4,64]{1,0:T(4,128)} %bitcast.5, f32[4,64]{1,0:T(4,128)} %bitcast.6, f32[1,2048]{1,0:T(1,128)} %bitcast.4, f32[1,512]{1,0:T(1,128)} %bitcast.7, bf16[2,2048,512]{2,1,0:T(8,128)(2,1)} %gate_hbm.1, bf16[2,2048,512]{2,1,0:T(8,128)(2,1)} %up_hbm.1, ...), custom_call_target="tpu_custom_call" | custom-call | tf_op jit(solution)/shard_map/pallas_call | solution.py:475
  26.2 0.6 %copy.10 = bf16[64,512]{1,0:T(8,128)(2,1)} copy(bf16[64,512]{1,0:T(8,128)(2,1)S(1)} %shard_map.82) | data formatting | bytes 131072

commit v4 on v3

--- a/solution.py
+++ b/solution.py
@@ -65,6 +65,7 @@
     ready,
     turn,
     sent_sem,
+    chip_sem,
     pair_recv,
     code_recv,
     chip_recv,
@@ -112,10 +113,11 @@
 
     sent = []
 
-    def start(src, dst, recv_sem, device):
-        copy = send(src, dst, sent_sem, recv_sem, device)
+    def start(src, dst, recv_sem, device, out_sem=sent_sem):
+        copy = send(src, dst, out_sem, recv_sem, device)
         copy.start()
-        sent.append(src)
+        if out_sem is sent_sem:
+            sent.append(src)
 
     def arrived(slot, sem):
         send(slot, slot, sent_sem, sem, {"ep": partner}).wait_recv()
@@ -279,16 +281,21 @@
     def own(k):
         return isinstance(k, int)
 
-    def project(step, k):
+    def project(step, group):
         index = chip_at(step)
         both = jnp.concatenate([hidden[2 * index + 1 - core], hidden[2 * index + core]], axis=0)
-        columns = pl.ds(pl.multiple_of(tp_at(k) * out_width, out_width), out_width)
-        out = jnp.dot(both, down_buf[:, columns], preferred_element_type=F32)
-        core_out[step, k] = out[:toks].astype(BF16)
-        core_sum[step, k] = out[toks:]
-        start(
-            core_out.at[step, k], core_in.at[step, k], core_recv.at[step, k], {"ep": partner}
-        )
+        for k in group:
+            columns = pl.ds(pl.multiple_of(tp_at(k) * out_width, out_width), out_width)
+            out = jnp.dot(both, down_buf[:, columns], preferred_element_type=F32)
+            core_out[step, k] = out[:toks].astype(BF16)
+            core_sum[step, k] = out[toks:]
+        for k in group:
+            start(
+                core_out.at[step, k],
+                core_in.at[step, k],
+                core_recv.at[step, k],
+                {"ep": partner},
+            )
 
     def crossed(step, k):
         block = core_in.at[step, k]
@@ -304,16 +311,25 @@
         else:
             near_sum[...] = total[:, cut:]
 
-    def other_chip(step, k):
-        total = crossed(step, k)
+    def send_chip(step, k):
         slot = step - 1
-        chip_out[k, slot] = total[:, :cut].astype(BF16)
         start(
             chip_out.at[k, slot],
             chip_in.at[k, slot],
             red_recv.at[k, slot],
             {"ep": 2 * chip_at(step) + core},
+            chip_sem,
         )
+
+    def other_chip(step, k):
+        total = crossed(step, k)
+        slot = step - 1
+        chip_out[k, slot] = total[:, :cut].astype(BF16)
+
+        @pl.when(core == 0)
+        def _():
+            send_chip(step, k)
+
         if not own(k):
             late_out[slot, k - 1] = total[:, cut:].astype(BF16)
             start(
@@ -335,34 +351,23 @@
     if tp_size > 2:
         learn(0)
     loaded(down_buf, experts)
-    for i, k in enumerate(order):
-        project(0, k)
-        if i == len(order) // 4 - 1:
-            forward(2)
-            forward(3)
-        if i == 3 * len(order) // 4 - 1:
-            forward(4)
-            forward(5)
-    forward(6)
-    forward(7)
+    project(0, order[: tp_size // 2])
+    for j in range(2, 5):
+        forward(j)
+    project(0, order[tp_size // 2 :])
+    for j in range(5, 8):
+        forward(j)
+    for j in range(8, direct):
+        forward(j)
     for r in range(1, tp_size - 2):
         learn(r)
     for k in order:
         own_chip(k)
-    for j in range(8, direct):
-        forward(j)
     if chips > 1:
         arrived(codes.at[pl.ds(0, ep_size - 2)], code_recv.at[1])
 
-    def sides():
-        for j in range(PIECES - 1, direct - 1, -1):
-            forward(j)
-
-    marked = len(sent)
-
-    @pl.when(core == 1)
-    def _():
-        sides()
+    for j in range(PIECES - 1, direct - 1, -1):
+        forward(j)
 
     for step in range(1, chips):
         index = chip_at(chips - step)
@@ -373,28 +378,26 @@
             if number == 0:
                 mix = mixes(index)
             other_experts(index, number, mix)
-            if number == 0 and step == 1:
-
-                @pl.when(core == 0)
-                def _():
-                    sides()
-
-                del sent[marked:]
-                sent.extend([rows.at[me, 0]] * (SIDE * (chips - 1)))
+
+        project(chips - step, order[: tp_size // 2])
+        project(chips - step, order[tp_size // 2 :])
 
         for k in order:
-            project(chips - step, k)
+            other_chip(chips - step, k)
+
+        @pl.when(core == 0)
+        def _():
+            for k in order:
+                src = chip_out.at[k, chips - step - 1]
+                send(src, src, chip_sem, chip_sem, {"ep": partner}).wait_send()
+            pl.semaphore_signal(turn, inc=1, device_id={"ep": partner}, device_id_type=MESH)
 
         @pl.when(core == 1)
         def _():
             pl.semaphore_wait(turn, 1)
-
-        for k in order:
-            other_chip(chips - step, k)
-
-        @pl.when(core == 0)
-        def _():
-            pl.semaphore_signal(turn, inc=1, device_id={"ep": partner}, device_id_type=MESH)
+            for k in order:
+                send_chip(chips - step, k)
+
 
     def reduced(k):
         total = own_sum[k]
@@ -410,19 +413,35 @@
 
     for k in order[:-2]:
         own_features(k)
-    for slot in range(chips - 1):
-        total = late_sum[slot]
-        arrived(late_in.at[slot], late_recv.at[slot])
-        for k in range(1, tp_size):
-            total = total + late_in[slot, k - 1].astype(F32)
-        back_out[slot] = total.astype(BF16)
-        start(
-            back_out.at[slot],
-            back_in.at[slot],
-            back_recv,
-            {"ep": 2 * chip_at(slot + 1) + core},
-        )
-    own_features(order[-2])
+
+    def add_late():
+        for slot in range(chips - 1):
+            total = late_sum[slot]
+            arrived(late_in.at[slot], late_recv.at[slot])
+            for k in range(1, tp_size):
+                total = total + late_in[slot, k - 1].astype(F32)
+            back_out[slot] = total.astype(BF16)
+            start(
+                back_out.at[slot],
+                back_in.at[slot],
+                back_recv,
+                {"ep": 2 * chip_at(slot + 1) + core},
+            )
+
+    marked = len(sent)
+
+    @pl.when(tp < tp_size // 2)
+    def _():
+        own_features(order[-2])
+        add_late()
+
+    @pl.when(tp >= tp_size // 2)
+    def _():
+        add_late()
+        own_features(order[-2])
+
+    del sent[marked:]
+    sent += [feat_out.at[0]] + [back_out.at[slot] for slot in range(chips - 1)]
     left = reduced(0)
     right = near_sum[...]
     arrived(early_in, early_recv)
@@ -455,6 +474,13 @@
     factor = lax.rsqrt(total / width + EPS)
     smalls[4].wait()
     out_ref[...] = (mixed * factor * out_gain_ref[...]).astype(BF16)
+    @pl.when(core == 1)
+    def _():
+        for step in range(1, chips):
+            for k in order:
+                src = chip_out.at[k, step - 1]
+                send(src, src, chip_sem, chip_sem, {"ep": partner}).wait_send()
+
     for src in sent:
         send(src, src, sent_sem, sent_sem, {"ep": partner}).wait_send()
 
@@ -513,6 +539,7 @@
             pltpu.SemaphoreType.REGULAR,
             dma,
             dma,
+            dma,
             dma((2,)),
             dma((chips - 1, PIECES - SIDE)),
             dma((chips - 1, SIDE)),

time: 26.9 us -> 26.5 us (0.985)
  Pallas kernels: 26.2 us -> 25.7 us
    pallas_call x1, Pallas kernels: 26.2 us -> 25.7 us  [on_device(): pl.pallas_call(functools.partial(kernel, ep_size, tp_size), out_shape=plt...]
where the time goes in v4:
time: 26.5 us; the launch traced here: 26.4 us
  Pallas kernels  25.7 us (97%)
  local copies, waits for them, and re-layouts  0.63 us (2%)
    pallas_call x1, Pallas kernels, on_device(): pl.pallas_call(functools.partial(kernel, ep_size, tp_size), out_shape=plt...  25.7 us
    unnamed x1, local copies, waits for them, and re-layouts  0.63 us

profile of v4, /device:TPU:0, one launch (start us, length us, event | category | flops | bytes accessed | tf_op | source)
XLA Modules:
  0.0 26.4 jit_solution(12976696540413914877)
XLA Ops:
  0.0 25.7 %shard_map.82 = bf16[64,512]{1,0:T(8,128)(2,1)S(1)} custom-call(bf16[64,2048]{1,0:T(8,128)(2,1)} %tok_hbm.1, s32[4,64]{1,0:T(4,128)} %bitcast.5, f32[4,64]{1,0:T(4,128)} %bitcast.6, f32[1,2048]{1,0:T(1,128)} %bitcast.4, f32[1,512]{1,0:T(1,128)} %bitcast.7, bf16[2,2048,512]{2,1,0:T(8,128)(2,1)} %gate_hbm.1, bf16[2,2048,512]{2,1,0:T(8,128)(2,1)} %up_hbm.1, ...), custom_call_target="tpu_custom_call" | custom-call | tf_op jit(solution)/shard_map/pallas_call | solution.py:501
  25.7 0.6 %copy.10 = bf16[64,512]{1,0:T(8,128)(2,1)} copy(bf16[64,512]{1,0:T(8,128)(2,1)S(1)} %shard_map.82) | data formatting | bytes 131072

commit v5 on v4

--- a/solution.py
+++ b/solution.py
@@ -14,6 +14,7 @@
 PIECES = 16
 SIDE = 4
 CHUNKS = ((0, 8), (8, 12), (12, 16))
+GROUPS = ((0, 1), (1, 1), (2, 1), (3, 1), (4, 4), (8, 4))
 MESH = pl.DeviceIdType.MESH
 BF16 = jnp.bfloat16
 F32 = jnp.float32
@@ -71,6 +72,7 @@
     chip_recv,
     side_recv,
     fwd_recv,
+    own_recv,
     core_recv,
     red_recv,
     early_recv,
@@ -91,7 +93,6 @@
     out_width = width // tp_size
     cut = out_width // 2
     depth = width // PIECES
-    direct = PIECES - SIDE
 
     chip_table = [lax.rem(chip + step, chips) for step in range(chips)]
 
@@ -180,19 +181,15 @@
 
     pl.semaphore_wait(barrier, ep_size - 1 + beside_count)
 
-    def piece(slot, j):
-        return rows.at[slot, j + odd * (PIECES - 1 - 2 * j)]
-
-    def send_pieces():
-        for j in range(direct):
-            for step in range(1, chips):
-                block = piece(me, j)
-                slot = chip_recv.at[step - 1, j]
-                start(block, block, slot, {"ep": 2 * chip_at(step) + core})
+    def pieces(slot, first, count):
+        return rows.at[slot, pl.ds(first + odd * (PIECES - 2 * first - count), count)]
 
     start(rows.at[me], rows.at[me], pair_recv, {"ep": partner})
-
-    send_pieces()
+    for g, (first, count) in enumerate(GROUPS):
+        for step in range(1, chips):
+            block = pieces(me, first, count)
+            start(block, block, chip_recv.at[step - 1, g], {"ep": 2 * chip_at(step) + core})
+
     if tp_size > 2:
         tell(ready.at[0])
 
@@ -259,16 +256,17 @@
                 for i in range(2):
                     acc[e, i] = sums[i]
 
-    def forward(j):
-        number = [a <= j < b for a, b in CHUNKS].index(True)
+    def forward(g):
+        first, count = GROUPS[g] if g < len(GROUPS) else (PIECES - SIDE, SIDE)
+        number = [a <= first < b for a, b in CHUNKS].index(True)
         for step in range(1, chips):
-            block = piece(2 * chip_at(chips - step) + core, j)
-            if j < direct:
-                arrived(block, chip_recv.at[step - 1, j])
+            block = pieces(2 * chip_at(chips - step) + core, first, count)
+            if g < len(GROUPS):
+                arrived(block, chip_recv.at[step - 1, g])
             else:
-                arrived(block, side_recv.at[step - 1, j - direct])
-            if j < SIDE:
-                start(block, block, side_recv.at[step - 1, SIDE - 1 - j], beside)
+                arrived(block, side_recv.at[step - 1])
+            if g < SIDE:
+                start(block, block, side_recv.at[step - 1], beside)
             start(block, block, fwd_recv.at[step - 1, number], {"ep": partner})
 
     order = [0] * (tp_size - 1)
@@ -293,14 +291,14 @@
             start(
                 core_out.at[step, k],
                 core_in.at[step, k],
-                core_recv.at[step, k],
+                core_recv.at[step - 1, k] if step else own_recv,
                 {"ep": partner},
             )
 
     def crossed(step, k):
-        block = core_in.at[step, k]
-        arrived(block, core_recv.at[step, k])
-        return core_sum[step, k] + block[...].astype(F32)
+        if step:
+            arrived(core_in.at[step, k], core_recv.at[step - 1, k])
+        return core_sum[step, k] + core_in[step, k].astype(F32)
 
     def own_chip(k):
         total = crossed(0, k)
@@ -352,23 +350,19 @@
         learn(0)
     loaded(down_buf, experts)
     project(0, order[: tp_size // 2])
-    for j in range(2, 5):
-        forward(j)
+    forward(2)
+    forward(3)
     project(0, order[tp_size // 2 :])
-    for j in range(5, 8):
-        forward(j)
-    for j in range(8, direct):
-        forward(j)
+    forward(4)
     for r in range(1, tp_size - 2):
         learn(r)
+    forward(5)
+    arrived(core_in.at[0], own_recv)
     for k in order:
         own_chip(k)
     if chips > 1:
         arrived(codes.at[pl.ds(0, ep_size - 2)], code_recv.at[1])
-
-    for j in range(PIECES - 1, direct - 1, -1):
-        forward(j)
-
+    forward(6)
     for step in range(1, chips):
         index = chip_at(chips - step)
         for number, (a, b) in enumerate(CHUNKS):
@@ -379,15 +373,15 @@
                 mix = mixes(index)
             other_experts(index, number, mix)
 
-        project(chips - step, order[: tp_size // 2])
-        project(chips - step, order[tp_size // 2 :])
+        for k in order:
+            project(chips - step, [k])
 
         for k in order:
             other_chip(chips - step, k)
 
         @pl.when(core == 0)
         def _():
-            for k in order:
+            for k in order[:3]:
                 src = chip_out.at[k, chips - step - 1]
                 send(src, src, chip_sem, chip_sem, {"ep": partner}).wait_send()
             pl.semaphore_signal(turn, inc=1, device_id={"ep": partner}, device_id_type=MESH)
@@ -428,20 +422,8 @@
                 {"ep": 2 * chip_at(slot + 1) + core},
             )
 
-    marked = len(sent)
-
-    @pl.when(tp < tp_size // 2)
-    def _():
-        own_features(order[-2])
-        add_late()
-
-    @pl.when(tp >= tp_size // 2)
-    def _():
-        add_late()
-        own_features(order[-2])
-
-    del sent[marked:]
-    sent += [feat_out.at[0]] + [back_out.at[slot] for slot in range(chips - 1)]
+    own_features(order[-2])
+    add_late()
     left = reduced(0)
     right = near_sum[...]
     arrived(early_in, early_recv)
@@ -474,12 +456,19 @@
     factor = lax.rsqrt(total / width + EPS)
     smalls[4].wait()
     out_ref[...] = (mixed * factor * out_gain_ref[...]).astype(BF16)
+    def left_over(ks):
+        for step in range(1, chips):
+            for k in ks:
+                src = chip_out.at[k, step - 1]
+                send(src, src, chip_sem, chip_sem, {"ep": partner}).wait_send()
+
     @pl.when(core == 1)
     def _():
-        for step in range(1, chips):
-            for k in order:
-                src = chip_out.at[k, step - 1]
-                send(src, src, chip_sem, chip_sem, {"ep": partner}).wait_send()
+        left_over(order)
+
+    @pl.when(core == 0)
+    def _():
+        left_over(order[3:])
 
     for src in sent:
         send(src, src, sent_sem, sent_sem, {"ep": partner}).wait_send()
@@ -541,10 +530,11 @@
             dma,
             dma,
             dma((2,)),
-            dma((chips - 1, PIECES - SIDE)),
-            dma((chips - 1, SIDE)),
+            dma((chips - 1, len(GROUPS))),
+            dma((chips - 1,)),
             dma((chips - 1, len(CHUNKS))),
-            dma((chips, tp_size)),
+            dma,
+            dma((chips - 1, tp_size)),
             dma((tp_size, chips - 1)),
             dma,
             dma((chips - 1,)),

time: 26.5 us -> 26.3 us (level)
  no operation moved by 1% of the time
where the time goes in v5:
time: 26.3 us; the launch traced here: 26.1 us
  Pallas kernels  25.5 us (97%)
  local copies, waits for them, and re-layouts  0.63 us (2%)
    pallas_call x1, Pallas kernels, on_device(): pl.pallas_call(functools.partial(kernel, ep_size, tp_size), out_shape=plt...  25.5 us
    unnamed x1, local copies, waits for them, and re-layouts  0.63 us

profile of v5, /device:TPU:0, one launch (start us, length us, event | category | flops | bytes accessed | tf_op | source)
XLA Modules:
  0.0 26.1 jit_solution(6115635026148314309)
XLA Ops:
  0.0 25.5 %shard_map.82 = bf16[64,512]{1,0:T(8,128)(2,1)S(1)} custom-call(bf16[64,2048]{1,0:T(8,128)(2,1)} %tok_hbm.1, s32[4,64]{1,0:T(4,128)} %bitcast.5, f32[4,64]{1,0:T(4,128)} %bitcast.6, f32[1,2048]{1,0:T(1,128)} %bitcast.4, f32[1,512]{1,0:T(1,128)} %bitcast.7, bf16[2,2048,512]{2,1,0:T(8,128)(2,1)} %gate_hbm.1, bf16[2,2048,512]{2,1,0:T(8,128)(2,1)} %up_hbm.1, ...), custom_call_target="tpu_custom_call" | custom-call | tf_op jit(solution)/shard_map/pallas_call | solution.py:490
  25.5 0.6 %copy.10 = bf16[64,512]{1,0:T(8,128)(2,1)} copy(bf16[64,512]{1,0:T(8,128)(2,1)S(1)} %shard_map.82) | data formatting | bytes 131072

commit v6 on v5

--- a/solution.py
+++ b/solution.py
@@ -369,9 +369,9 @@
             first = a + odd * (PIECES - a - b)
             block = rows.at[2 * index + 1 - core, pl.ds(first, b - a)]
             arrived(block, fwd_recv.at[step - 1, number])
+            other_experts(index, number, None if number == 0 else mix)
             if number == 0:
                 mix = mixes(index)
-            other_experts(index, number, mix)
 
         for k in order:
             project(chips - step, [k])
@@ -432,16 +432,19 @@
     arrived(feat_in, feat_recv)
     for k in range(1, tp_size):
         left = left + feat_in[k - 1].astype(F32)
+    def fold(part):
+        squares = part * part
+        total = squares[:, :LANES]
+        for j in range(1, part.shape[1] // LANES):
+            total = total + squares[:, j * LANES : (j + 1) * LANES]
+        return total
+
+    folded = fold(left)
     if chips > 1:
         arrived(back_in, back_recv)
     for slot in range(chips - 1):
         right = right + back_in[slot].astype(F32)
-    mixed = jnp.concatenate([left, right], axis=1)
-
-    squares = mixed * mixed
-    folded = jnp.zeros((toks, LANES), F32)
-    for j in range(out_width // LANES):
-        folded = folded + squares[:, j * LANES : (j + 1) * LANES]
+    folded = folded + fold(right)
     wide = square_out.shape[1]
     if wide > toks:
         folded = jnp.concatenate([folded, jnp.zeros((wide - toks, LANES), F32)], axis=0)
@@ -449,13 +452,14 @@
     square_out[...] = jnp.broadcast_to(line, square_out.shape)
     for k in range(1, tp_size):
         start(square_out, square_in.at[k - 1], sq_recv, {"tp": tp_at(k)})
+    smalls[4].wait()
+    mixed = jnp.concatenate([left, right], axis=1) * out_gain_ref[...]
     arrived(square_in, sq_recv)
     for k in range(1, tp_size):
         line = line + square_in[k - 1, 0:1, :]
     total = jnp.broadcast_to(line, (LANES, wide)).T[:toks, :1]
     factor = lax.rsqrt(total / width + EPS)
-    smalls[4].wait()
-    out_ref[...] = (mixed * factor * out_gain_ref[...]).astype(BF16)
+    out_ref[...] = (mixed * factor).astype(BF16)
     def left_over(ks):
         for step in range(1, chips):
             for k in ks:

time: 26.3 us -> 26.3 us (level)
  no operation moved by 1% of the time
where the time goes in v6:
time: 26.3 us; the launch traced here: 26.1 us
  Pallas kernels  25.5 us (97%)
  local copies, waits for them, and re-layouts  0.63 us (2%)
    pallas_call x1, Pallas kernels, on_device(): pl.pallas_call(functools.partial(kernel, ep_size, tp_size), out_shape=plt...  25.5 us
    unnamed x1, local copies, waits for them, and re-layouts  0.63 us

profile of v6, /device:TPU:0, one launch (start us, length us, event | category | flops | bytes accessed | tf_op | source)
XLA Modules:
  0.0 26.1 jit_solution(9692152161513586032)
XLA Ops:
  0.0 25.5 %shard_map.82 = bf16[64,512]{1,0:T(8,128)(2,1)S(1)} custom-call(bf16[64,2048]{1,0:T(8,128)(2,1)} %tok_hbm.1, s32[4,64]{1,0:T(4,128)} %bitcast.5, f32[4,64]{1,0:T(4,128)} %bitcast.6, f32[1,2048]{1,0:T(1,128)} %bitcast.4, f32[1,512]{1,0:T(1,128)} %bitcast.7, bf16[2,2048,512]{2,1,0:T(8,128)(2,1)} %gate_hbm.1, bf16[2,2048,512]{2,1,0:T(8,128)(2,1)} %up_hbm.1, ...), custom_call_target="tpu_custom_call" | custom-call | tf_op jit(solution)/shard_map/pallas_call | solution.py:494
  25.5 0.6 %copy.10 = bf16[64,512]{1,0:T(8,128)(2,1)} copy(bf16[64,512]{1,0:T(8,128)(2,1)S(1)} %shard_map.82) | data formatting | bytes 131072
